TPU v7x, 32 devices: a whole 2x2x4 slice. The times are simulated.
32 devices in a mesh: sp: 2 (over x), tp: 16 (over z, y, core).
Axes of the slice: x: 2, y: 2, z: 4, core: 2. Of those that a mesh axis runs over, the one named last changes fastest.
Arguments:
- query_first: bfloat16 [1024, 1536], P('sp', 'tp'), may hold values from -10 to 10
- query_second: bfloat16 [1024, 2560], P('sp', 'tp'), may hold values from -10 to 10
- latent: bfloat16 [1024, 512], P('sp'), may hold values from -400 to 400
- key_rotary: bfloat16 [1024, 32], P('sp'), may hold values from -90 to 90
- latent_gain: float32 [512], replicated, may hold values from 0.1 to 1.9
- key_up_first: bfloat16 [512, 1024], P(None, 'tp'), may hold values from -0.25 to 0.25
- value_up_first: bfloat16 [512, 1024], P(None, 'tp'), may hold values from -0.25 to 0.25
- key_up_second: bfloat16 [512, 2048], P(None, 'tp'), may hold values from -0.25 to 0.25
- value_up_second: bfloat16 [512, 2048], P(None, 'tp'), may hold values from -0.25 to 0.25
- out_first: bfloat16 [1024, 2048], P('tp'), may hold values from -0.109375 to 0.109375
- out_second: bfloat16 [2048, 2048], P('tp'), may hold values from -0.109375 to 0.109375
- residual: bfloat16 [1024, 2048], P('sp'), may hold values from -16 to 16
- expert_gain: float32 [2048], replicated, may hold values from 0.1 to 1.9
- route_experts: int32 [1024, 2], P('sp'), may hold values from 0 to 31, all different within a row; in each aligned block of 32 rows (0 to 31, 32 to 63, ...) at most 3 rows name the same one
- route_scores: float32 [1024, 2], P('sp'), may hold values from -6 to 306
- gate_weight: bfloat16 [32, 2048, 4096], P('sp', None, 'tp'), may hold values from -0.375 to 0.375
- up_weight: bfloat16 [32, 2048, 4096], P('sp', None, 'tp'), may hold values from -0.375 to 0.375
- down_weight: bfloat16 [32, 4096, 2048], P('sp', 'tp'), may hold values from -0.013671875 to 0.013671875
Outputs:
- mixed: bfloat16 [1024, 2048], P(('sp', 'tp'))
Inputs may be any that keep to these rules, and one draw needn't show every extreme that they name: `route_experts`: each row names 2 different experts. In every aligned block of 32 rows no expert is named more than 3 times, and in some blocks one is named exactly 3 times.
All inputs are finite; a program needn't handle non-finite values.
Results may differ from a plain program's by a relative error of at most 0.02.
The roundings to bfloat16 on the way count: a program that leaves them out, or rounds other values in their place, can miss the bound.
Values may be sent and summed in bfloat16 or wider, within the bound.
A program may use at most 128 MiB of HBM per device.

v0:
```python
import jax
import jax.numpy as jnp
from jax import lax
from jax.sharding import PartitionSpec as P

NA = 64
NB = 128
ROPE = 32
CAP = 3


norm_epsilon = 1e-06
rotary_base = 10000.0
clamp_limit = 7.0
sigmoid_slope = 1.702
masked_score = -1e30


def rotate(values, positions):
    half = values.shape[-1] // 2
    inverse = rotary_base ** (-jnp.arange(half, dtype=jnp.float32) / half)
    angles = positions.astype(jnp.float32)[:, None, None] * inverse[None, None, :]
    cosine = jnp.cos(angles)
    sine = jnp.sin(angles)
    first = values[..., :half]
    second = values[..., half:]
    return jnp.concatenate(
        [first * cosine - second * sine, second * cosine + first * sine], axis=-1
    )


def rms_scaled(values, gain):
    wide = values.astype(jnp.float32)
    return wide * lax.rsqrt(jnp.mean(wide * wide, axis=-1, keepdims=True) + norm_epsilon) * gain


def turned_queries(query, nope, positions):
    shaped = query.reshape(query.shape[0], query.shape[1] // (nope + ROPE), nope + ROPE)
    turned = rotate(shaped[..., nope:].astype(jnp.float32), positions).astype(jnp.bfloat16)
    return jnp.concatenate([shaped[..., :nope], turned], axis=-1)


def clamped_unit(gate, upward):
    limited = jnp.minimum(gate, clamp_limit)
    bounded = jnp.clip(upward, -clamp_limit, clamp_limit)
    return (bounded + 1.0) * limited * jax.nn.sigmoid(sigmoid_slope * limited)


def slot_numbers(chosen, experts):
    hits = (chosen[..., None] == jnp.arange(experts, dtype=jnp.int32)).astype(jnp.int32)
    before = jnp.cumsum(hits, axis=-2) - hits
    return chosen * CAP + jnp.sum(before * hits, axis=-1)


def fold_group(state, queries, key_nope, key_turned, values, query_places, scale):
    running, denominator, numerator = state
    heads = queries.shape[1]
    nope = queries.shape[2] - key_turned.shape[1]
    keys = key_nope.reshape(key_nope.shape[0], heads, nope)
    value_rows = values.reshape(values.shape[0], heads, values.shape[1] // heads)
    score = jnp.einsum(
        "qhd,khd->qhk", queries[..., :nope], keys, preferred_element_type=jnp.float32
    )
    score = score + jnp.einsum(
        "qhr,kr->qhk", queries[..., nope:], key_turned, preferred_element_type=jnp.float32
    )
    score = score * scale
    key_places = jnp.arange(keys.shape[0], dtype=jnp.int32)
    allowed = (query_places[:, None] >= key_places[None, :])[:, None, :]
    score = jnp.where(allowed, score, masked_score)
    highest = jnp.maximum(running, jnp.max(score, axis=-1))
    weights = jnp.where(allowed, jnp.exp(score - highest[..., None]), 0.0)
    denominator = jnp.sum(weights, axis=-1)
    numerator = jnp.einsum(
        "qhk,khd->qhd", weights.astype(jnp.bfloat16), value_rows, preferred_element_type=jnp.float32
    )
    return (highest, denominator, numerator)


def expert_hidden(rows, gate_weight, up_weight):
    gate = jnp.einsum("nsecd,edf->nsecf", rows, gate_weight, preferred_element_type=jnp.float32)
    upward = jnp.einsum("nsecd,edf->nsecf", rows, up_weight, preferred_element_type=jnp.float32)
    return clamped_unit(gate, upward).astype(jnp.bfloat16)


def body(
    query_first,
    query_second,
    latent,
    key_rotary,
    latent_gain,
    key_up_first,
    value_up_first,
    key_up_second,
    value_up_second,
    out_first,
    out_second,
    residual,
    expert_gain,
    route_experts,
    route_scores,
    gate_weight,
    up_weight,
    down_weight,
):
    seq_rows = latent.shape[0]
    sets = lax.axis_size("tp")
    groups = lax.axis_size("sp")
    own_rows = seq_rows // sets
    topk = route_experts.shape[1]
    local_experts = gate_weight.shape[0]
    experts = local_experts * groups
    offset = lax.axis_index("sp") * seq_rows
    places = offset + jnp.arange(seq_rows, dtype=jnp.int32)
    last_place = offset + seq_rows - 1
    queries_first = turned_queries(query_first, NA, places)
    queries_second = turned_queries(query_second, NB, places)
    key_turned = rotate(key_rotary.astype(jnp.float32)[:, None, :], places)[:, 0, :].astype(
        jnp.bfloat16
    )
    latent_normed = rms_scaled(latent, latent_gain).astype(jnp.bfloat16)
    scale_first = (NA + ROPE) ** (-0.5)
    scale_second = (NB + ROPE) ** (-0.5)

    def attend(carry, parts):
        key_first, value_first, key_second, value_second, turned = parts
        return (
            fold_group(
                carry[0], queries_first, key_first, turned, value_first, places, scale_first
            ),
            fold_group(
                carry[1], queries_second, key_second, turned, value_second, places, scale_second
            ),
        )

    def initial(queries, value_width):
        shape = queries.shape[:2]
        return (
            jnp.full(shape, masked_score, jnp.float32),
            jnp.zeros(shape, jnp.float32),
            jnp.zeros(shape + (value_width,), jnp.float32),
        )

    start_state = (
        initial(queries_first, value_up_first.shape[1] // queries_first.shape[1]),
        initial(queries_second, value_up_second.shape[1] // queries_second.shape[1]),
    )
    key_first, value_first, key_second, value_second = tuple(
        (
            jnp.dot(latent_normed, weight, preferred_element_type=jnp.float32).astype(jnp.bfloat16)
            for weight in (key_up_first, value_up_first, key_up_second, value_up_second)
        )
    )
    parts = (
        lax.all_gather(key_first, "sp", axis=0, tiled=True),
        lax.all_gather(value_first, "sp", axis=0, tiled=True),
        lax.all_gather(key_second, "sp", axis=0, tiled=True),
        lax.all_gather(value_second, "sp", axis=0, tiled=True),
        lax.all_gather(key_turned, "sp", axis=0, tiled=True),
    )
    state = lax.cond(
        jnp.int32(0) <= last_place,
        lambda inner: attend(inner, parts),
        lambda inner: inner,
        start_state,
    )
    first_state, second_state = state
    attended_first = (
        (first_state[2] / first_state[1][..., None]).astype(jnp.bfloat16).reshape(seq_rows, -1)
    )
    attended_second = (
        (second_state[2] / second_state[1][..., None]).astype(jnp.bfloat16).reshape(seq_rows, -1)
    )
    own_start = lax.axis_index("tp") * own_rows
    slot_range = jnp.arange(experts * CAP, dtype=jnp.int32)
    projected = lax.psum_scatter(
        (
            jnp.dot(attended_first, out_first, preferred_element_type=jnp.float32)
            + jnp.dot(attended_second, out_second, preferred_element_type=jnp.float32)
        ).astype(jnp.bfloat16),
        "tp",
        scatter_dimension=0,
        tiled=True,
    ).astype(jnp.float32)
    own_residual = lax.dynamic_slice_in_dim(residual, own_start, own_rows, 0)
    middle = (own_residual.astype(jnp.float32) + projected).astype(jnp.bfloat16)
    normed = rms_scaled(middle, expert_gain).astype(jnp.bfloat16)
    own_ids = lax.dynamic_slice_in_dim(route_experts, own_start, own_rows, 0).reshape(-1)
    own_slots = slot_numbers(own_ids, experts)
    picks = (own_slots[:, None] == slot_range).reshape(own_rows, topk, experts * CAP)
    selected = jnp.sum(picks.astype(jnp.float32), axis=1).astype(jnp.bfloat16)
    outgoing = jnp.einsum("ts,td->sd", selected, normed, preferred_element_type=jnp.float32).astype(
        jnp.bfloat16
    )
    outgoing = outgoing.reshape(groups, local_experts, CAP, outgoing.shape[-1])
    arrived = lax.all_to_all(outgoing, "sp", split_axis=0, concat_axis=0, tiled=True)
    activated = expert_hidden(
        lax.all_gather(arrived[None], "tp", axis=0, tiled=True), gate_weight, up_weight
    )
    flat_hidden = activated.reshape(sets * groups, local_experts, CAP, activated.shape[-1])
    summed = lax.psum_scatter(
        jnp.einsum(
            "secf,efd->secd", flat_hidden, down_weight, preferred_element_type=jnp.float32
        ).astype(jnp.bfloat16),
        "tp",
        scatter_dimension=0,
        tiled=True,
    )
    returned = lax.all_to_all(summed, "sp", split_axis=0, concat_axis=0, tiled=True)
    expert_out = returned.reshape(experts * CAP, returned.shape[-1]).astype(jnp.float32)
    own_scores = lax.dynamic_slice_in_dim(route_scores, own_start, own_rows, 0)
    route_weight = jax.nn.softmax(own_scores, axis=-1)
    matches = own_slots.reshape(own_rows, topk)[..., None] == slot_range
    combine = jnp.sum(jnp.where(matches, route_weight[..., None], 0.0), axis=1)
    mixture = jnp.dot(combine, expert_out, precision=lax.Precision.HIGHEST)
    return (middle.astype(jnp.float32) + mixture).astype(jnp.bfloat16)


def solution(mesh):
    in_specs = (
        P("sp", "tp"),
        P("sp", "tp"),
        P("sp", None),
        P("sp", None),
        P(),
        P(None, "tp"),
        P(None, "tp"),
        P(None, "tp"),
        P(None, "tp"),
        P("tp", None),
        P("tp", None),
        P("sp", None),
        P(),
        P("sp", None),
        P("sp", None),
        P("sp", None, "tp"),
        P("sp", None, "tp"),
        P("sp", "tp", None),
    )
    out_specs = P(("sp", "tp"), None)
    return jax.shard_map(body, mesh=mesh, in_specs=in_specs, out_specs=out_specs, check_vma=False)
```

profile of v0, /device:TPU:0, one launch (start us, length us, event | category | flops | bytes accessed | tf_op | source)
XLA Modules:
  0.0 321.1 jit_solution(14557094529585508583)
XLA Ops:
  6.7 1.3 fusion.46
  8.0 1.5 convolution_convert_fusion.3
  9.5 5.9 %all_gather.20 = bf16[1024,64]{0,1:T(8,128)(2,1)S(1)} all-gather(bf16[512,64]{0,1:T(8,128)(2,1)S(1)} %convolution_convert_fusion.3), channel_id=1, replica_groups=mesh['sp'=2,'tp'=16] {'sp'}, dimensions={0}, use_global_device_ids=true | all-gather | bytes 196608 | tf_op jit(solution)/shard_map/all_gather | solution.py:156
  15.3 1.4 convolution_convert_fusion.4
  16.8 4.9 %all_gather.18 = bf16[1024,64]{0,1:T(8,128)(2,1)S(1)} all-gather(bf16[512,64]{0,1:T(8,128)(2,1)S(1)} %convolution_convert_fusion.4), channel_id=1, replica_groups=mesh['sp'=2,'tp'=16] {'sp'}, dimensions={0}, use_global_device_ids=true | all-gather | bytes 196608 | tf_op jit(solution)/shard_map/all_gather | solution.py:155
  22.0 4.6 %all-gather = bf16[1024,1,32]{0,2,1:T(8,128)(2,1)S(1)} all-gather(bf16[512,1,32]{0,2,1:T(8,128)(2,1)S(1)} %pad_maximum_fusion.1), channel_id=2, replica_groups=mesh['sp'=2,'tp'=16] {'sp'}, dimensions={0}, use_global_device_ids=true | all-gather | bytes 98304 | tf_op jit(solution)/shard_map/all_gather | solution.py:159
  27.4 6.9 %all_gather.22 = bf16[1024,128]{1,0:T(8,128)(2,1)S(1)} all-gather(bf16[512,128]{1,0:T(8,128)(2,1)S(1)} %convolution_convert_fusion.1), channel_id=1, replica_groups=mesh['sp'=2,'tp'=16] {'sp'}, dimensions={0}, use_global_device_ids=true | all-gather | bytes 393216 | tf_op jit(solution)/shard_map/all_gather | solution.py:158
  34.3 5.6 %all_gather.21 = bf16[1024,128]{1,0:T(8,128)(2,1)S(1)} all-gather(bf16[512,128]{1,0:T(8,128)(2,1)S(1)} %convolution_convert_fusion.2), channel_id=1, replica_groups=mesh['sp'=2,'tp'=16] {'sp'}, dimensions={0}, use_global_device_ids=true | all-gather | bytes 393216 | tf_op jit(solution)/shard_map/all_gather | solution.py:157
  39.9 4.2 %conditional.1 = (f32[512,1]{0,1:T(1,128)S(1)}, f32[512,1,64]{0,2,1:T(8,128)S(1)}, f32[512,1]{0,1:T(1,128)S(1)}, f32[512,1,128]{2,0,1:T(8,128)S(1)}) conditional(s32[]{:T(128)} %convert_element_type.116, () %tuple.13, (s32[]{:T(128)}, s32[512]{0:T(512)S(1)}, bf16[512,1,96]{0,2,1:T(8,128)(2,1)S(1)}, bf16[1024,64]{0,1:T(8,128)(2,1)S(1)}, ...), branch_computations={%region_1.0_spmd, %region_2.7_spmd} | conditional | flops 482868736 | bytes 22911012 | solution.py:161
  42.8 0.8 fusion.7
  44.1 0.8 fusion.54
  45.0 2.1 add_convert_fusion
  47.9 0.7 constant_dynamic-slice_fusion.1
  49.7 61.2 %reduce-scatter.3.cloned.1.call-done = bf16[32,2048]{1,0:T(8,128)(2,1)} async-done(((bf16[512,2048]{1,0:T(8,128)(2,1)}), bf16[32,2048]{1,0:T(8,128)(2,1)}) %reduce-scatter.3.cloned.1.call-update) | async-done | bytes 131088 | tf_op jit(solution)/shard_map/reduce_scatter | solution.py:176
  110.9 1.1 fusion.50
  112.9 9.0 %all_to_all.10 = bf16[2,16,3,2048]{3,1,2,0:T(8,128)(2,1)} all-to-all(bf16[2,16,3,2048]{3,1,2,0:T(8,128)(2,1)S(1)} %copy.80), channel_id=1, replica_groups=mesh['sp'=2,'tp'=16] {'sp'}, dimensions={0} | all-to-all | bytes 786432 | tf_op jit(solution)/shard_map/all_to_all | solution.py:196
  122.1 59.4 %all-gather.4.cloned.1.call-done = bf16[32,16,3,2048]{3,1,2,0:T(8,128)(2,1)} async-done(((bf16[2,16,3,2048]{3,1,2,0:T(8,128)(2,1)}), bf16[32,16,3,2048]{3,1,2,0:T(8,128)(2,1)}) %all-gather.4.cloned.1.call-update) | async-done | bytes 6291472 | tf_op jit(solution)/shard_map/all_gather | solution.py:198
  181.5 12.1 %fusion.30 = f32[16,16,2,3,256]{4,1,3,2,0:T(8,128)S(1)} fusion(bf16[16,2048,256]{2,1,0:T(8,128)(2,1)} %param.36, bf16[16,2,16,3,2048]{4,2,3,1,0:T(8,128)(2,1)} %bitcast.112), kind=kOutput, calls=%fused_computation.39 | convolution fusion | flops 1610612736 | bytes 24641536 | tf_op jit(solution)/shard_map/nsecd,edf->nsecf/dot_general | solution.py:82
  193.5 10.4 %fusion.41 = bf16[16,2,16,3,256]{4,0,3,1,2:T(8,128)(2,1)S(1)} fusion(bf16[16,2048,256]{2,1,0:T(8,128)(2,1)} %param.35, bf16[16,2,16,3,2048]{4,2,3,1,0:T(8,128)(2,1)S(1)} %bitcast.113, f32[16,16,2,3,256]{4,1,3,2,0:T(8,128)S(1)} %fusion.30), kind=kOutput, calls=%fused_computation.51 | convolution fusion | flops 1614544896 | bytes 25427968 | tf_op jit(solution)/shard_map/nsecd,edf->nsecf/dot_general | solution.py:81
  204.4 8.9 %convert_bitcast_fusion = bf16[32,16,3,2048]{3,0,2,1:T(8,128)(2,1)S(1)} fusion(bf16[16,256,2048]{2,1,0:T(8,128)(2,1)} %param.37, bf16[32,16,3,256]{3,1,2,0:T(8,128)(2,1)S(1)} %bitcast.114), kind=kOutput, calls=%fused_computation.41 | convolution fusion | flops 1613758464 | bytes 23855104 | tf_op jit(solution)/shard_map/secf,efd->secd/dot_general | solution.py:202
  213.3 6.1 %copy.85 = bf16[32,16,3,2048]{3,1,2,0:T(8,128)(2,1)} copy(bf16[32,16,3,2048]{3,0,2,1:T(8,128)(2,1)S(1)} %convert_bitcast_fusion) | data formatting | bytes 12582912 | tf_op jit(solution)/shard_map/convert_element_type | solution.py:204
  219.5 83.9 %reduce-scatter.5.cloned.1.call-done = bf16[2,16,3,2048]{3,1,2,0:T(8,128)(2,1)} async-done(((bf16[32,16,3,2048]{3,1,2,0:T(8,128)(2,1)}), bf16[2,16,3,2048]{3,1,2,0:T(8,128)(2,1)}) %reduce-scatter.5.cloned.1.call-update) | async-done | bytes 393232 | tf_op jit(solution)/shard_map/reduce_scatter | solution.py:201
  303.4 9.6 %all_to_all.11 = bf16[2,16,3,2048]{3,1,2,0:T(8,128)(2,1)S(1)} all-to-all(bf16[2,16,3,2048]{3,1,2,0:T(8,128)(2,1)} %reduce-scatter.5.cloned.1.call-done), channel_id=1, replica_groups=mesh['sp'=2,'tp'=16] {'sp'}, dimensions={0} | all-to-all | bytes 786432 | tf_op jit(solution)/shard_map/all_to_all | solution.py:209
  313.7 0.9 fusion.36
  (72 shorter events, 8.5 us)
Async XLA Ops:
  6.5 37.6 %copy-start = (bf16[128,2048]{1,0:T(8,128)(2,1)S(1)}, bf16[128,2048]{1,0:T(8,128)(2,1)}, u32[]{:S(2)}) copy-start(bf16[128,2048]{1,0:T(8,128)(2,1)} %param.30) | copy-start | bytes 1572868
  6.5 20.1 %copy-start.3 = (bf16[512,512]{1,0:T(8,128)(2,1)S(1)}, bf16[512,512]{1,0:T(8,128)(2,1)}, u32[]{:S(2)}) copy-start(bf16[512,512]{1,0:T(8,128)(2,1)} %param.22) | copy-start | bytes 1572868
  6.5 20.1 %copy-start.12 = (f32[512]{0:T(512)S(1)}, f32[512]{0:T(512)}, u32[]{:S(2)}) copy-start(f32[512]{0:T(512)} %param.24) | copy-start | bytes 6148
  6.5 15.2 %copy-start.6 = (bf16[512,96]{0,1:T(8,128)(2,1)S(1)}, bf16[512,96]{0,1:T(8,128)(2,1)}, u32[]{:S(2)}) copy-start(bf16[512,96]{0,1:T(8,128)(2,1)} %param.20) | copy-start | bytes 294916
  6.5 15.2 %copy-start.5 = (bf16[512,160]{0,1:T(8,128)(2,1)S(1)}, bf16[512,160]{0,1:T(8,128)(2,1)}, u32[]{:S(2)}) copy-start(bf16[512,160]{0,1:T(8,128)(2,1)} %param.21) | copy-start | bytes 491524
  6.5 15.2 %copy-start.7 = (bf16[512,32]{0,1:T(8,128)(2,1)S(1)}, bf16[512,32]{0,1:T(8,128)(2,1)}, u32[]{:S(2)}) copy-start(bf16[512,32]{0,1:T(8,128)(2,1)} %param.23) | copy-start | bytes 98308
  6.6 20.1 %copy-start.10 = (bf16[512,128]{1,0:T(8,128)(2,1)S(1)}, bf16[512,128]{1,0:T(8,128)(2,1)}, u32[]{:S(2)}) copy-start(bf16[512,128]{1,0:T(8,128)(2,1)} %param.27) | copy-start | bytes 393220
  6.6 104.3 %reduce-scatter.3.cloned.1.call-start = ((), (), s32[]{:S(2)}) async-start(), calls=%async_computation.4 | async-start | bytes 2228224 | tf_op jit(solution)/shard_map/reduce_scatter | solution.py:176
  8.0 19.0 %copy-start.11 = (bf16[512,128]{1,0:T(8,128)(2,1)S(1)}, bf16[512,128]{1,0:T(8,128)(2,1)}, u32[]{:S(2)}) copy-start(bf16[512,128]{1,0:T(8,128)(2,1)} %param.28) | copy-start | bytes 393220
  44.1 1.0 copy-start.4
  47.1 0.7 copy-start.9
  47.1 64.9 %copy-start.8 = (f32[2048]{0:T(1024)S(1)}, f32[2048]{0:T(1024)}, u32[]{:S(2)}) copy-start(f32[2048]{0:T(1024)} %param.32) | copy-start | bytes 24580
  47.2 134.3 %all-gather.4.cloned.1.call-start = ((), (), s32[]{:S(2)}) async-start(), calls=%async_computation.6 | async-start | bytes 6684672 | tf_op jit(solution)/shard_map/all_gather | solution.py:198
  121.9 181.5 %reduce-scatter.5.cloned.1.call-start = ((), (), s32[]{:S(2)}) async-start(), calls=%async_computation.5 | async-start | bytes 6684672 | tf_op jit(solution)/shard_map/reduce_scatter | solution.py:201
  181.5 12.1 %copy-start.2 = (bf16[32,16,3,2048]{3,1,2,0:T(8,128)(2,1)S(1)}, bf16[32,16,3,2048]{3,1,2,0:T(8,128)(2,1)}, u32[]{:S(2)}) copy-start(bf16[32,16,3,2048]{3,1,2,0:T(8,128)(2,1)} %all-gather.4.cloned.1.call-done) | copy-start | bytes 18874372
  219.5 95.2 %copy-start.1 = (bf16[128,2048]{1,0:T(8,128)(2,1)S(1)}, bf16[128,2048]{1,0:T(8,128)(2,1)}, u32[]{:S(2)}) copy-start(bf16[128,2048]{1,0:T(8,128)(2,1)} %param.30) | copy-start | bytes 1572868
Sparse Core Ops, SparseCore 0:
  47.3 63.5 reduce-scatter.2
  122.0 59.4 all-gather.3
  219.6 83.7 reduce-scatter.4
where the time goes:
time: 322 us; the launch traced here: 321 us
  waiting for transfers between devices  204 us (63%)
  blocking collectives  46.5 us (14%)
  matrix products  42.3 us (13%)
  between operations  13.4 us (4%)
  local copies, waits for them, and re-layouts  9.84 us (3%)
  other arithmetic  4.28 us (1%)
    reduce_scatter x1, waiting for transfers between devices, body(): lax.psum_scatter(jnp.einsum('secf,efd->secd', flat_hidden, down_weight, p...  83.9 us
    reduce_scatter x1, waiting for transfers between devices, body(): lax.psum_scatter((jnp.dot(attended_first, out_first, preferred_element_ty...  61.2 us
    all_gather x1, waiting for transfers between devices, body(): lax.all_gather(arrived[None], 'tp', axis=0, tiled=True)  59.4 us
    dot_general x1, matrix products, expert_hidden(): jnp.einsum('nsecd,edf->nsecf', rows, up_weight, preferred_element_type=jn...  12.1 us
    dot_general x1, matrix products, expert_hidden(): jnp.einsum('nsecd,edf->nsecf', rows, gate_weight, preferred_element_type=...  10.4 us
    all_to_all x1, blocking collectives, body(): lax.all_to_all(summed, 'sp', split_axis=0, concat_axis=0, tiled=True)  9.59 us
    all_to_all x1, blocking collectives, body(): lax.all_to_all(outgoing, 'sp', split_axis=0, concat_axis=0, tiled=True)  8.98 us
    dot_general x1, matrix products, body(): jnp.einsum('secf,efd->secd', flat_hidden, down_weight, preferred_element_...  8.89 us
  transfers between devices with their start and end apart: 3, of which 3 were waited for; matrix products, arithmetic and copies ran while one was open for 1% of the time, Pallas kernels for 0%

commit v1 on v0

--- a/solution.py
+++ b/solution.py
@@ -1,6 +1,10 @@
+import functools
+
 import jax
 import jax.numpy as jnp
 from jax import lax
+from jax.experimental import pallas as pl
+from jax.experimental.pallas import tpu as pltpu
 from jax.sharding import PartitionSpec as P
 
 NA = 64
@@ -83,7 +87,7 @@
     return clamped_unit(gate, upward).astype(jnp.bfloat16)
 
 
-def body(
+def slot_body(
     query_first,
     query_second,
     latent,
@@ -216,6 +220,481 @@
     return (middle.astype(jnp.float32) + mixture).astype(jnp.bfloat16)
 
 
+MESH = pl.DeviceIdType.MESH
+VMEM = pl.BlockSpec(memory_space=pltpu.VMEM)
+TILE_TOKENS = 256
+
+
+def places_of(axes):
+    return {axis: lax.axis_index(axis) for axis in axes}
+
+
+def bit_of(place, step):
+    axis, mask = step
+    return (place[axis] // mask) % 2
+
+
+def partner_of(place, step):
+    axis, mask = step
+    return {axis: place[axis] + mask * (1 - 2 * bit_of(place, step))}
+
+
+def greet(place, steps):
+    barrier = pltpu.get_barrier_semaphore()
+    for step in steps:
+        pl.semaphore_signal(
+            barrier, inc=1, device_id=partner_of(place, step), device_id_type=MESH
+        )
+    pl.semaphore_wait(barrier, len(steps))
+
+
+def cube_steps(sp, tp):
+    core = [("tp", 1)] if tp > 1 else []
+    first = [("tp", 2)] if tp > 2 else []
+    rest = [("tp", 1 << i) for i in range(2, tp.bit_length() - 1)]
+    across = [("sp", 1 << i) for i in range(sp.bit_length() - 1)]
+    return core, first, rest, across
+
+
+def weight_of(step, widths):
+    axis, mask = step
+    return mask * (widths if axis == "sp" else 1)
+
+
+def base_of(place, fixed, width):
+    total = jnp.int32(0)
+    for step in fixed:
+        total = total + bit_of(place, step) * weight_of(step, width)
+    return total
+
+
+def offsets_of(free, width):
+    found = [0]
+    for step in free:
+        found = found + [one + weight_of(step, width) for one in found]
+    return found
+
+
+def block_rows_of(index, rows):
+    return pl.ds(pl.multiple_of(index * rows, rows), rows)
+
+
+def gather_kernel(orders, width, x_ref, out_ref, send_sem, recv_sem, own_sem):
+    place = places_of(("sp", "tp"))
+    steps = orders[0]
+    rows = x_ref.shape[0]
+    cols = x_ref.shape[1] // len(orders)
+    greet(place, steps)
+    own = pltpu.make_async_copy(
+        x_ref, out_ref.at[block_rows_of(base_of(place, steps, width), rows), :], own_sem
+    )
+    own.start()
+
+    def columns(part):
+        return pl.ds(part * cols, cols)
+
+    def start(part, number):
+        order = orders[part]
+        base = base_of(place, order[number:], width)
+        for offset in offsets_of(order[:number], width):
+            spot = out_ref.at[block_rows_of(base + offset, rows), columns(part)]
+            source = x_ref.at[:, columns(part)] if number == 0 else spot
+            pltpu.make_async_remote_copy(
+                src_ref=source,
+                dst_ref=spot,
+                send_sem=send_sem.at[part, number],
+                recv_sem=recv_sem.at[part, number],
+                device_id=partner_of(place, order[number]),
+                device_id_type=MESH,
+            ).start()
+
+    def drain(part, number, sem):
+        whole = out_ref.at[pl.ds(0, rows << number), columns(part)]
+        pltpu.make_async_copy(whole, whole, sem.at[part, number]).wait()
+
+    for part in range(len(orders)):
+        start(part, 0)
+    own.wait()
+    for wave in range(len(steps) + 1):
+        for part in range(len(orders)):
+            number = wave - part // 2 % 2
+            if number < 0 or number >= len(steps):
+                continue
+            drain(part, number, recv_sem)
+            if number + 1 < len(steps):
+                start(part, number + 1)
+    for part in range(len(orders)):
+        for number in range(len(steps)):
+            drain(part, number, send_sem)
+
+
+def gather_blocks(x, orders, width, count, collective_id):
+    rows, depth = x.shape
+    parts, stages = len(orders), len(orders[0])
+    return pl.pallas_call(
+        functools.partial(gather_kernel, orders, width),
+        out_shape=jax.ShapeDtypeStruct((rows * count, depth), x.dtype),
+        in_specs=[VMEM],
+        out_specs=VMEM,
+        scratch_shapes=[
+            pltpu.SemaphoreType.DMA((parts, stages)),
+            pltpu.SemaphoreType.DMA((parts, stages)),
+            pltpu.SemaphoreType.DMA,
+        ],
+        compiler_params=pltpu.CompilerParams(
+            collective_id=collective_id, has_side_effects=True, vmem_limit_bytes=40 << 20
+        ),
+        name="gather_blocks",
+    )(x)
+
+
+def scatter_kernel(
+    orders, width, rows, x_ref, out_ref, total_ref, landing_ref, send_sem, recv_sem
+):
+    place = places_of(("sp", "tp"))
+    stages = len(orders[0])
+    cols = x_ref.shape[1] // len(orders)
+    greet(place, orders[0])
+    spots = [0]
+    for number in range(stages):
+        spots.append(spots[-1] + (1 << (stages - 1 - number)))
+
+    def columns(part):
+        return pl.ds(part * cols, cols)
+
+    def start(part, number):
+        order = orders[part]
+        step = order[number]
+        source = x_ref if number == 0 else total_ref
+        base = base_of(place, order[:number], width)
+        base = base + (1 - bit_of(place, step)) * weight_of(step, width)
+        for slot, offset in enumerate(offsets_of(order[number + 1 :], width)):
+            pltpu.make_async_remote_copy(
+                src_ref=source.at[block_rows_of(base + offset, rows), columns(part)],
+                dst_ref=landing_ref.at[pl.ds((spots[number] + slot) * rows, rows), columns(part)],
+                send_sem=send_sem.at[part, number],
+                recv_sem=recv_sem.at[part, number],
+                device_id=partner_of(place, step),
+                device_id_type=MESH,
+            ).start()
+
+    def drain(part, number, sem):
+        count = 1 << (stages - 1 - number)
+        whole = landing_ref.at[pl.ds(spots[number] * rows, count * rows), columns(part)]
+        pltpu.make_async_copy(whole, whole, sem.at[part, number]).wait()
+
+    def add(part, number):
+        order = orders[part]
+        source = x_ref if number == 0 else total_ref
+        base = base_of(place, order[: number + 1], width)
+        for slot, offset in enumerate(offsets_of(order[number + 1 :], width)):
+            here = block_rows_of(base + offset, rows)
+            there = pl.ds((spots[number] + slot) * rows, rows)
+            value = source[here, columns(part)].astype(jnp.float32) + landing_ref[
+                there, columns(part)
+            ].astype(jnp.float32)
+            if number + 1 < stages:
+                total_ref[here, columns(part)] = value.astype(total_ref.dtype)
+            else:
+                out_ref[:, columns(part)] = value
+
+    for part in range(len(orders)):
+        start(part, 0)
+    for wave in range(stages + 1):
+        for part in range(len(orders)):
+            number = wave - part // 2 % 2
+            if number < 0 or number >= stages:
+                continue
+            drain(part, number, recv_sem)
+            add(part, number)
+            if number + 1 < stages:
+                start(part, number + 1)
+    for part in range(len(orders)):
+        for number in range(stages):
+            drain(part, number, send_sem)
+
+
+def scatter_blocks(x, orders, width, count, collective_id):
+    rows = x.shape[0] // count
+    depth = x.shape[1]
+    parts, stages = len(orders), len(orders[0])
+    return pl.pallas_call(
+        functools.partial(scatter_kernel, orders, width, rows),
+        out_shape=jax.ShapeDtypeStruct((rows, depth), jnp.float32),
+        in_specs=[VMEM],
+        out_specs=VMEM,
+        scratch_shapes=[
+            pltpu.VMEM(x.shape, x.dtype),
+            pltpu.VMEM(((count - 1) * rows, depth), x.dtype),
+            pltpu.SemaphoreType.DMA((parts, stages)),
+            pltpu.SemaphoreType.DMA((parts, stages)),
+        ],
+        compiler_params=pltpu.CompilerParams(
+            collective_id=collective_id, has_side_effects=True, vmem_limit_bytes=40 << 20
+        ),
+        name="scatter_blocks",
+    )(x)
+
+
+def exchange_kernel(latent_ref, turn_ref, route_ref, l_out, t_out, r_out, send_sem, recv_sem, own_sem):
+    place = places_of(("sp", "tp"))
+    across, core = ("sp", 1), ("tp", 1)
+    greet(place, (across, core))
+    half = latent_ref.shape[0] // 2
+    side = bit_of(place, core)
+    me = place["sp"]
+    other = 1 - me
+    pairs = ((latent_ref, l_out), (turn_ref, t_out))
+    mine = pl.ds(pl.multiple_of(side * half, half), half)
+    crossing = []
+    for number, (source, target) in enumerate(pairs):
+        crossing.append(
+            pltpu.make_async_remote_copy(
+                src_ref=source.at[mine, :],
+                dst_ref=target.at[me, mine, :],
+                send_sem=send_sem.at[number],
+                recv_sem=recv_sem.at[number],
+                device_id=partner_of(place, across),
+                device_id_type=MESH,
+            )
+        )
+    crossing.append(
+        pltpu.make_async_remote_copy(
+            src_ref=route_ref,
+            dst_ref=r_out.at[me],
+            send_sem=send_sem.at[2],
+            recv_sem=recv_sem.at[2],
+            device_id=partner_of(place, across),
+            device_id_type=MESH,
+        )
+    )
+    for copy in crossing:
+        copy.start()
+    kept = [
+        pltpu.make_async_copy(source, target.at[me], own_sem.at[number])
+        for number, (source, target) in enumerate(pairs + ((route_ref, r_out),))
+    ]
+    for copy in kept:
+        copy.start()
+    passing = []
+    for number, (source, target) in enumerate(pairs):
+        crossing[number].wait_recv()
+        spot = target.at[other, mine, :]
+        copy = pltpu.make_async_remote_copy(
+            src_ref=spot,
+            dst_ref=spot,
+            send_sem=send_sem.at[3 + number],
+            recv_sem=recv_sem.at[3 + number],
+            device_id=partner_of(place, core),
+            device_id_type=MESH,
+        )
+        copy.start()
+        passing.append(copy)
+    crossing[2].wait_recv()
+    for copy in crossing:
+        copy.wait_send()
+    for copy in kept + passing:
+        copy.wait()
+
+
+def exchange(latent, turn, route, collective_id):
+    return pl.pallas_call(
+        exchange_kernel,
+        out_shape=tuple(
+            jax.ShapeDtypeStruct((2,) + one.shape, one.dtype) for one in (latent, turn, route)
+        ),
+        in_specs=[VMEM] * 3,
+        out_specs=(VMEM,) * 3,
+        scratch_shapes=[
+            pltpu.SemaphoreType.DMA((5,)),
+            pltpu.SemaphoreType.DMA((5,)),
+            pltpu.SemaphoreType.DMA((3,)),
+        ],
+        compiler_params=pltpu.CompilerParams(collective_id=collective_id, has_side_effects=True),
+        name="exchange",
+    )(latent, turn, route)
+
+
+def expert_kernel(pitch, x_ref, code_ref, gate_ref, up_ref, down_ref, out_ref, rows_ref, scale_ref):
+    index = pl.program_id(0)
+    experts = pl.num_programs(0)
+    tiles, count, _, depth = rows_ref.shape
+    span = count * pitch
+    tokens = x_ref.shape[0] // tiles
+
+    def hits(tile, choice):
+        wanted = code_ref[tile, pl.ds(choice, 1), :]
+        slots = lax.broadcasted_iota(jnp.int32, (span, tokens), 0)
+        return slots == wanted.astype(jnp.int32)
+
+    @pl.when(index == 0)
+    def _():
+        for tile in range(tiles):
+            first, second = hits(tile, 0), hits(tile, 1)
+            chosen = jnp.where(first | second, 1.0, 0.0).astype(jnp.bfloat16)
+            picked = jnp.dot(
+                chosen,
+                x_ref[pl.ds(tile * tokens, tokens), :],
+                preferred_element_type=jnp.float32,
+            ).astype(jnp.bfloat16)
+            rows_ref[tile] = picked.reshape(count, pitch, depth)
+            share = jnp.where(first, code_ref[tile, pl.ds(2, 1), :], 0.0) + jnp.where(
+                second, code_ref[tile, pl.ds(3, 1), :], 0.0
+            )
+            scale_ref[tile] = jnp.sum(share, axis=1, keepdims=True).reshape(count, pitch, 1)
+
+    rows = rows_ref[:, index].reshape(tiles * pitch, depth)
+    gate = jnp.dot(rows, gate_ref[0], preferred_element_type=jnp.float32)
+    upward = jnp.dot(rows, up_ref[0], preferred_element_type=jnp.float32)
+    activated = clamped_unit(gate, upward).astype(jnp.bfloat16)
+    result = jnp.dot(activated, down_ref[0], preferred_element_type=jnp.float32)
+    scaled = result * scale_ref[:, index].reshape(tiles * pitch, 1)
+    rows_ref[:, index] = scaled.astype(jnp.bfloat16).reshape(tiles, pitch, depth)
+
+    @pl.when(index == experts - 1)
+    def _():
+        for tile in range(tiles):
+            chosen = jnp.where(hits(tile, 0) | hits(tile, 1), 1.0, 0.0).astype(jnp.bfloat16)
+            out_ref[pl.ds(tile * tokens, tokens), :] = lax.dot_general(
+                chosen,
+                rows_ref[tile].reshape(span, depth),
+                (((0,), (0,)), ((), ())),
+                preferred_element_type=jnp.float32,
+            ).astype(jnp.bfloat16)
+
+
+def run_experts(tokens, codes, gate_weight, up_weight, down_weight, pitch):
+    experts, depth, units = gate_weight.shape
+    tiles = codes.shape[0]
+    return pl.pallas_call(
+        functools.partial(expert_kernel, pitch),
+        grid=(experts,),
+        out_shape=jax.ShapeDtypeStruct(tokens.shape, jnp.bfloat16),
+        in_specs=[
+            pl.BlockSpec(tokens.shape, lambda i: (0, 0)),
+            pl.BlockSpec(codes.shape, lambda i: (0, 0, 0)),
+            pl.BlockSpec((1, depth, units), lambda i: (i, 0, 0)),
+            pl.BlockSpec((1, depth, units), lambda i: (i, 0, 0)),
+            pl.BlockSpec((1, units, depth), lambda i: (i, 0, 0)),
+        ],
+        out_specs=pl.BlockSpec(tokens.shape, lambda i: (0, 0)),
+        scratch_shapes=[
+            pltpu.VMEM((tiles, experts, pitch, depth), jnp.bfloat16),
+            pltpu.VMEM((tiles, experts, pitch, 1), jnp.float32),
+        ],
+        compiler_params=pltpu.CompilerParams(
+            dimension_semantics=("arbitrary",), vmem_limit_bytes=56 << 20
+        ),
+        name="run_experts",
+    )(tokens, codes, gate_weight, up_weight, down_weight)
+
+
+def attended_heads(queries, nope, keys, turned, values, allowed, scale):
+    heads = queries.shape[1]
+    wide = keys.reshape(keys.shape[0], heads, nope)
+    shared = jnp.broadcast_to(turned[:, None, :], (turned.shape[0], heads, turned.shape[1]))
+    whole = jnp.concatenate([wide, shared], axis=-1)
+    value_rows = values.reshape(values.shape[0], heads, values.shape[1] // heads)
+    score = jnp.einsum("qhd,khd->hqk", queries, whole, preferred_element_type=jnp.float32) * scale
+    score = jnp.where(allowed, score, masked_score)
+    highest = jnp.max(score, axis=-1, keepdims=True)
+    weights = jnp.exp(score - highest)
+    denominator = jnp.sum(weights, axis=-1)
+    numerator = jnp.einsum(
+        "hqk,khd->hqd", weights.astype(jnp.bfloat16), value_rows, preferred_element_type=jnp.float32
+    )
+    attended = (numerator / denominator[..., None]).astype(jnp.bfloat16)
+    return jnp.swapaxes(attended, 0, 1).reshape(attended.shape[1], -1)
+
+
+def token_body(
+    query_first,
+    query_second,
+    latent,
+    key_rotary,
+    latent_gain,
+    key_up_first,
+    value_up_first,
+    key_up_second,
+    value_up_second,
+    out_first,
+    out_second,
+    residual,
+    expert_gain,
+    route_experts,
+    route_scores,
+    gate_weight,
+    up_weight,
+    down_weight,
+):
+    seq_rows = latent.shape[0]
+    sets = lax.axis_size("tp")
+    groups = lax.axis_size("sp")
+    own_rows = seq_rows // sets
+    local_experts = gate_weight.shape[0]
+    total = groups * seq_rows
+    me = lax.axis_index("sp")
+    core, first, rest, across = cube_steps(groups, sets)
+    span_blocks = TILE_TOKENS // own_rows
+    pitch = -(-span_blocks * CAP // 16) * 16
+
+    chosen = route_experts.reshape(sets, -1)
+    earlier = jnp.tril(jnp.ones((chosen.shape[1],) * 2, jnp.float32), -1)
+    same = (chosen[:, :, None] == chosen[:, None, :]).astype(jnp.float32)
+    rank = jnp.sum(same * earlier, axis=-1)
+    spot = ((jnp.arange(sets, dtype=jnp.int32) % span_blocks) * CAP).astype(jnp.float32)
+    code = chosen.astype(jnp.float32) * pitch + spot[:, None] + rank
+    code = code.reshape(seq_rows, -1).T
+    share = jax.nn.softmax(route_scores, axis=-1).T
+    route = jnp.concatenate([code, share, code, share], axis=0)
+
+    latents, turns, routes = exchange(latent, key_rotary, route, 0)
+
+    places = me * seq_rows + jnp.arange(seq_rows, dtype=jnp.int32)
+    all_places = jnp.arange(total, dtype=jnp.int32)
+    queries_first = turned_queries(query_first, NA, places)
+    queries_second = turned_queries(query_second, NB, places)
+    turned = rotate(
+        turns.reshape(total, -1).astype(jnp.float32)[:, None, :], all_places
+    )[:, 0, :].astype(jnp.bfloat16)
+    latent_normed = rms_scaled(latents.reshape(total, -1), latent_gain).astype(jnp.bfloat16)
+    key_first, value_first, key_second, value_second = tuple(
+        jnp.dot(latent_normed, weight, preferred_element_type=jnp.float32).astype(jnp.bfloat16)
+        for weight in (key_up_first, value_up_first, key_up_second, value_up_second)
+    )
+    allowed = (places[:, None] >= all_places[None, :])[None]
+    attended_first = attended_heads(
+        queries_first, NA, key_first, turned, value_first, allowed, (NA + ROPE) ** (-0.5)
+    )
+    attended_second = attended_heads(
+        queries_second, NB, key_second, turned, value_second, allowed, (NB + ROPE) ** (-0.5)
+    )
+    partial = (
+        jnp.dot(attended_first, out_first, preferred_element_type=jnp.float32)
+        + jnp.dot(attended_second, out_second, preferred_element_type=jnp.float32)
+    ).astype(jnp.bfloat16)
+    one, two = tuple(core + first + rest), tuple(core + rest + first)
+    projected = scatter_blocks(partial, (one, two, one, one), sets, sets, 1)
+    own_start = lax.axis_index("tp") * own_rows
+    own_residual = lax.dynamic_slice_in_dim(residual, own_start, own_rows, 0)
+    middle = (own_residual.astype(jnp.float32) + projected).astype(jnp.bfloat16)
+    normed = rms_scaled(middle, expert_gain).astype(jnp.bfloat16)
+    ladder = rest[::-1]
+    one = tuple(ladder + across + first + core)
+    two = tuple(ladder + first + across + core)
+    tokens = gather_blocks(normed, (one, two, one, two), sets, groups * sets, 2)
+
+    tiles = total // TILE_TOKENS
+    codes = jnp.swapaxes(routes, 0, 1).reshape(8, total)
+    shift = jnp.array([1.0, 1.0, 0.0, 0.0, 1.0, 1.0, 0.0, 0.0], jnp.float32)
+    codes = codes - (shift * (me * local_experts * pitch).astype(jnp.float32))[:, None]
+    codes = jnp.swapaxes(codes.reshape(8, tiles, TILE_TOKENS), 0, 1)
+    mixed = run_experts(tokens, codes, gate_weight, up_weight, down_weight, pitch)
+    one, two = one[::-1], two[::-1]
+    mixture = scatter_blocks(mixed, (one, two, one, two), sets, groups * sets, 3)
+    return (middle.astype(jnp.float32) + mixture).astype(jnp.bfloat16)
+
+
 def solution(mesh):
     in_specs = (
         P("sp", "tp"),
@@ -238,4 +717,11 @@
         P("sp", "tp", None),
     )
     out_specs = P(("sp", "tp"), None)
+    groups, sets = mesh.shape["sp"], mesh.shape["tp"]
+    small = groups == 2 and sets & (sets - 1) == 0 and sets > 2
+
+    def body(*arguments):
+        fits = small and arguments[2].shape[0] * groups <= 1024
+        return (token_body if fits else slot_body)(*arguments)
+
     return jax.shard_map(body, mesh=mesh, in_specs=in_specs, out_specs=out_specs, check_vma=False)

time: 322 us -> 174 us (0.54)
  waiting for transfers between devices: 204 us -> 0 us
  Pallas kernels: 0 us -> 140 us
  blocking collectives: 46.5 us -> 0 us
  matrix products: 42.3 us -> 8.7 us
  between operations: 13.4 us -> 0.3 us
  other arithmetic: 4.28 us -> 12.1 us
    reduce_scatter x2 -> x0, waiting for transfers between devices: 145 us -> none  [the longest x1 83.9 us: body(): lax.psum_scatter(jnp.einsum('secf,efd->secd', flat_hidden, down_weight, p...]
    pallas_call x0 -> x5, Pallas kernels: none -> 140 us  [the longest x2 61.4 us: scatter_blocks(): pl.pallas_call(functools.partial(scatter_kernel, orders, width, rows), ou...]
    all_gather x1 -> x0, waiting for transfers between devices: 59.4 us -> none  [body(): lax.all_gather(arrived[None], 'tp', axis=0, tiled=True)]
    dot_general x17 -> x8, matrix products: 42.3 us -> 8.7 us  [the longest x2 5.09 us: attended_heads(): jnp.einsum('hqk,khd->hqd', weights.astype(jnp.bfloat16), value_rows, pref...]
    all_gather x5 -> x0, blocking collectives: 27.9 us -> none  [the longest x1 6.89 us: body(): lax.all_gather(value_second, 'sp', axis=0, tiled=True)]
    all_to_all x2 -> x0, blocking collectives: 18.6 us -> none  [the longest x1 9.59 us: body(): lax.all_to_all(summed, 'sp', split_axis=0, concat_axis=0, tiled=True)]
    unnamed x27 -> x37, local copies, waits for them, and re-layouts: 0.93 us -> 9.79 us
    convert_element_type x2 -> x0, local copies, waits for them, and re-layouts: 6.55 us -> none  [the longest x1 6.11 us: body(): summed = lax.psum_scatter(jnp.einsum('secf,efd->secd', flat_hidden, down_...]
  transfers between devices with their start and end apart: 3 -> 0, of which waited for: 3 -> 0; matrix products, arithmetic and copies ran while one was open for 1% -> 0% of each run, Pallas kernels for 0% -> 0%
where the time goes in v1:
time: 174 us
  Pallas kernels  140 us (80%)
  local copies, waits for them, and re-layouts  12.4 us (7%)
  other arithmetic  12.1 us (7%)
  matrix products  8.7 us (5%)
    pallas_call x2, Pallas kernels, scatter_blocks(): pl.pallas_call(functools.partial(scatter_kernel, orders, width, rows), ou...  61.4 us
    pallas_call x1, Pallas kernels, gather_blocks(): pl.pallas_call(functools.partial(gather_kernel, orders, width), out_shape...  32.5 us
    pallas_call x1, Pallas kernels, run_experts(): pl.pallas_call(functools.partial(expert_kernel, pitch), grid=(experts,),...  31.5 us
    pallas_call x1, Pallas kernels, exchange(): pl.pallas_call(exchange_kernel, out_shape=tuple((jax.ShapeDtypeStruct((2,...  14.8 us
    unnamed x37, local copies, waits for them, and re-layouts  9.79 us
    dot_general x2, matrix products, attended_heads(): jnp.einsum('hqk,khd->hqd', weights.astype(jnp.bfloat16), value_rows, pref...  5.09 us

profile of v1, /device:TPU:0, one launch (start us, length us, event | category | flops | bytes accessed | tf_op | source)
XLA Modules:
  0.0 173.7 jit_solution(11379890254088947899)
XLA Ops:
  0.0 0.7 broadcast_multiply_fusion
  0.8 0.7 reduce_max.27
  1.5 0.7 fusion.61
  2.4 0.9 slice.40
  3.3 0.9 slice.46
  4.2 1.5 copy.30.turn_ref
  5.7 0.8 slice_convert_fusion
  6.7 0.8 copy.28
  9.1 14.8 %exchange.1 = (bf16[2,512,512]{2,1,0:T(8,128)(2,1)}, bf16[2,512,32]{2,1,0:T(8,128)(2,1)}, f32[2,8,512]{2,1,0:T(8,128)}) custom-call(bf16[512,512]{1,0:T(8,128)(2,1)} %latent_ref.1, bf16[512,32]{1,0:T(8,128)(2,1)} %copy.30.turn_ref, f32[8,512]{1,0:T(8,128)} %pad_maximum_fusion.route_ref), custom_call_target="tpu_custom_call" | custom-call | tf_op jit(solution)/shard_map/exchange/pallas_call | solution.py:501
  23.9 1.4 subtract_bitcast_fusion.code_ref
  25.4 1.5 multiply_reduce_fusion
  27.0 1.6 fusion.1
  31.1 1.3 copy-done.5
  33.0 2.7 %fusion.9 = bf16[512,128]{1,0:T(8,128)(2,1)S(1)} fusion(bf16[1024,512]{1,0:T(8,128)(2,1)S(1)} %fusion.1, bf16[512,128]{1,0:T(8,128)(2,1)S(1)} %copy-done.15, f32[512,1024]{1,0:T(8,128)} %copy-done.5, f32[512]{0:T(512)S(1)} %get-tuple-element.23, f32[512]{0:T(512)S(1)} %fusion.4), kind=kOutput, calls=%fused_computation.19 | convolution fusion | flops 269746176 | bytes 3411968 | tf_op jit(solution)/shard_map/hqk,khd->hqd/dot_general | solution.py:603
  36.3 1.4 copy-done.4
  38.2 2.4 %fusion.11 = bf16[512,64]{0,1:T(8,128)(2,1)S(1)} fusion(bf16[1024,512]{1,0:T(8,128)(2,1)S(1)} %fusion.1, bf16[512,64]{0,1:T(8,128)(2,1)S(1)} %copy-done.10, f32[512,1024]{1,0:T(8,128)} %copy-done.4, f32[512]{0:T(512)S(1)} %get-tuple-element.25, f32[512]{0:T(512)S(1)} %fusion.2), kind=kOutput, calls=%fused_computation.24 | convolution fusion | flops 135397376 | bytes 3280896 | tf_op jit(solution)/shard_map/hqk,khd->hqd/dot_general | solution.py:603
  41.5 0.7 add_convert_fusion.x_ref
  42.3 25.1 %scatter_blocks.2 = f32[32,2048]{1,0:T(8,128)S(1)} custom-call(bf16[512,2048]{1,0:T(8,128)(2,1)S(1)} %add_convert_fusion.x_ref), custom_call_target="tpu_custom_call" | custom-call | tf_op jit(solution)/shard_map/scatter_blocks/pallas_call | solution.py:421
  67.4 1.1 fusion.20
  68.6 32.5 %gather_blocks.1.x_ref = bf16[1024,2048]{1,0:T(8,128)(2,1)S(1)} custom-call(bf16[32,2048]{1,0:T(8,128)(2,1)S(1)} %fusion.22.x_ref), custom_call_target="tpu_custom_call" | custom-call | tf_op jit(solution)/shard_map/gather_blocks/pallas_call | solution.py:334
  101.1 1.9 %copy-done.2 = bf16[1024,2048]{1,0:T(8,128)(2,1)} copy-done((bf16[1024,2048]{1,0:T(8,128)(2,1)}, bf16[1024,2048]{1,0:T(8,128)(2,1)S(1)}, u32[]{:S(2)}) %copy-start.2) | copy-done | bytes 4194328
  103.0 31.5 %run_experts.1.x_ref = bf16[1024,2048]{1,0:T(8,128)(2,1)} custom-call(bf16[1024,2048]{1,0:T(8,128)(2,1)} %copy-done.2, f32[4,8,256]{2,1,0:T(8,128)} %subtract_bitcast_fusion.code_ref, bf16[16,2048,256]{2,1,0:T(8,128)(2,1)} %gate_ref.1, bf16[16,2048,256]{2,1,0:T(8,128)(2,1)} %up_ref.1, bf16[16,256,2048]{2,1,0:T(8,128)(2,1)} %down_ref.1), custom_call_target="tpu_custom_call" | custom-call | tf_op jit(solution)/shard_map/run_experts/pallas_call | solution.py:569
  134.5 2.2 %copy-done.3 = bf16[1024,2048]{1,0:T(8,128)(2,1)S(1)} copy-done((bf16[1024,2048]{1,0:T(8,128)(2,1)S(1)}, bf16[1024,2048]{1,0:T(8,128)(2,1)}, u32[]{:S(2)}) %copy-start.3) | copy-done | bytes 4194328
  136.7 36.3 %scatter_blocks.3 = f32[32,2048]{1,0:T(8,128)S(1)} custom-call(bf16[1024,2048]{1,0:T(8,128)(2,1)S(1)} %copy-done.3), custom_call_target="tpu_custom_call" | custom-call | tf_op jit(solution)/shard_map/scatter_blocks/pallas_call | solution.py:421
  (60 shorter events, 7.9 us)
Async XLA Ops:
  0.0 40.5 %copy-start = (bf16[128,2048]{1,0:T(8,128)(2,1)S(1)}, bf16[128,2048]{1,0:T(8,128)(2,1)}, u32[]{:S(2)}) copy-start(bf16[128,2048]{1,0:T(8,128)(2,1)} %param.29) | copy-start | bytes 1572868
  0.0 8.5 %copy-start.11 = (f32[512,2]{0,1:T(2,128)S(1)}, f32[512,2]{0,1:T(2,128)}, u32[]{:S(2)}) copy-start(f32[512,2]{0,1:T(2,128)} %param.33) | copy-start | bytes 12292
  0.0 8.5 %copy-start.12 = (s32[512,2]{0,1:T(2,128)S(1)}, s32[512,2]{0,1:T(2,128)}, u32[]{:S(2)}) copy-start(s32[512,2]{0,1:T(2,128)} %param.32) | copy-start | bytes 12292
  0.0 26.9 %copy-start.14 = (f32[512]{0:T(512)S(1)}, f32[512]{0:T(512)}, u32[]{:S(2)}) copy-start(f32[512]{0:T(512)} %param.23) | copy-start | bytes 6148
  8.4 20.2 %copy-start.9 = (bf16[512,64]{0,1:T(8,128)(2,1)S(1)}, bf16[512,64]{0,1:T(8,128)(2,1)}, u32[]{:S(2)}) copy-start(bf16[512,64]{0,1:T(8,128)(2,1)} %param.24) | copy-start | bytes 196612
  25.4 3.6 %copy-start.8 = (bf16[512,128]{1,0:T(8,128)(2,1)S(1)}, bf16[512,128]{1,0:T(8,128)(2,1)}, u32[]{:S(2)}) copy-start(bf16[512,128]{1,0:T(8,128)(2,1)} %param.26) | copy-start | bytes 393220
  26.9 2.5 %copy-start.7 = (bf16[2,512,32]{2,1,0:T(8,128)(2,1)S(1)}, bf16[2,512,32]{2,1,0:T(8,128)(2,1)}, u32[]{:S(2)}) copy-start(bf16[2,512,32]{2,1,0:T(8,128)(2,1)} %get-tuple-element.9) | copy-start | bytes 196612
  31.1 1.4 copy-start.5
  31.1 1.9 %copy-start.15 = (bf16[512,128]{1,0:T(8,128)(2,1)S(1)}, bf16[512,128]{1,0:T(8,128)(2,1)}, u32[]{:S(2)}) copy-start(bf16[512,128]{1,0:T(8,128)(2,1)} %param.27) | copy-start | bytes 393220
  35.7 2.5 %copy-start.10 = (bf16[512,64]{0,1:T(8,128)(2,1)S(1)}, bf16[512,64]{0,1:T(8,128)(2,1)}, u32[]{:S(2)}) copy-start(bf16[512,64]{0,1:T(8,128)(2,1)} %param.25) | copy-start | bytes 196612
  36.3 1.4 copy-start.4
  40.6 1.0 copy-start.6
  42.2 26.2 %copy-start.13 = (f32[2048]{0:T(1024)S(1)}, f32[2048]{0:T(1024)}, u32[]{:S(2)}) copy-start(f32[2048]{0:T(1024)} %param.31) | copy-start | bytes 24580
  101.1 1.9 %copy-start.2 = (bf16[1024,2048]{1,0:T(8,128)(2,1)}, bf16[1024,2048]{1,0:T(8,128)(2,1)S(1)}, u32[]{:S(2)}) copy-start(bf16[1024,2048]{1,0:T(8,128)(2,1)S(1)} %gather_blocks.1.x_ref) | copy-start | bytes 12582916
  103.0 70.7 %copy-start.1 = (bf16[128,2048]{1,0:T(8,128)(2,1)S(1)}, bf16[128,2048]{1,0:T(8,128)(2,1)}, u32[]{:S(2)}) copy-start(bf16[128,2048]{1,0:T(8,128)(2,1)} %param.29) | copy-start | bytes 1572868
  134.5 2.2 %copy-start.3 = (bf16[1024,2048]{1,0:T(8,128)(2,1)S(1)}, bf16[1024,2048]{1,0:T(8,128)(2,1)}, u32[]{:S(2)}) copy-start(bf16[1024,2048]{1,0:T(8,128)(2,1)} %run_experts.1.x_ref) | copy-start | bytes 12582916
